TPU v7x, 32 devices: a whole 2x2x4 slice. The times are simulated.
32 devices in a mesh: sp: 4 (over y, x), tp: 8 (over z, core).
Axes of the slice: x: 2, y: 2, z: 4, core: 2. Of those that a mesh axis runs over, the one named last changes fastest.
Arguments:
- tokens: bfloat16 [3, 2048, 4096], P(None, 'sp', 'tp'), may hold values from -6 to 6
- new_token: bfloat16 [3, 1, 4096], P(None, None, 'tp'), may hold values from -6 to 6
- query_weight: bfloat16 [4096, 4096], P(None, 'tp'), may hold values from -0.09375 to 0.09375
- key_weight: bfloat16 [4096, 4096], P(None, 'tp'), may hold values from -0.09375 to 0.09375
- value_weight: bfloat16 [4096, 4096], P(None, 'tp'), may hold values from -0.09375 to 0.09375
- log_decay: float32 [64], P('tp'), may hold values from -0.034 to 0
Outputs:
- state: bfloat16 [3, 64, 64, 64], P(None, 'tp', 'sp')
- read: bfloat16 [3, 4096], P(None, 'tp')
All inputs are finite; a program needn't handle non-finite values.
Results may differ from a plain program's by a relative error of at most 0.012.
Values may be sent and summed in bfloat16 or wider, within the bound.
A program may use at most 64 MiB of HBM per device.

v0:
```python
import jax
import jax.numpy as jnp
from jax import lax
from jax.sharding import PartitionSpec as P

HD = 64


def rotate(values, positions):
    half_dim = values.shape[-1] // 2
    inverse = 10000.0 ** (-jnp.arange(half_dim, dtype=jnp.float32) / half_dim)
    angles = positions.astype(jnp.float32)[:, None, None] * inverse[None, None, :]
    cosine = jnp.cos(angles)
    sine_part = jnp.sin(angles)
    first = values[..., :half_dim]
    second = values[..., half_dim:]
    return jnp.concatenate(
        [first * cosine - second * sine_part, first * sine_part + second * cosine], axis=-1
    )


def group_norm(output):
    centered = output - jnp.mean(output, axis=-1, keepdims=True)
    return centered * lax.rsqrt(jnp.mean(centered * centered, axis=-1, keepdims=True) + 1e-05)


def body(tokens, new_token, query_weight, key_weight, value_weight, log_decay):
    sequences, span_len, _ = tokens.shape
    head_count = log_decay.shape[0]
    inner = head_count * HD
    groups = lax.axis_size("sp")
    own_index = lax.axis_index("sp")
    key_scale = HD ** (-0.5)
    key_share = HD // groups
    row_weights = jnp.concatenate([key_weight, value_weight], axis=1)
    all_weights = jnp.concatenate([key_weight, value_weight, query_weight], axis=1)
    row_piece = lax.all_gather(tokens, "tp", axis=2, tiled=True)
    new_piece = lax.all_gather(new_token, "tp", axis=2, tiled=True)
    row_total = jnp.dot(row_piece, row_weights, preferred_element_type=jnp.float32)
    new_total = jnp.dot(new_piece, all_weights, preferred_element_type=jnp.float32)
    row_total = row_total.reshape(sequences, span_len, 2, head_count, HD)
    offsets = own_index * span_len + jnp.arange(span_len, dtype=jnp.int32)
    key_rows = (rotate(row_total[:, :, 0], offsets) * key_scale).astype(jnp.bfloat16)
    value_rows = row_total[:, :, 1].astype(jnp.bfloat16)
    to_end = (span_len - 1 - jnp.arange(span_len, dtype=jnp.int32)).astype(jnp.float32)
    decay_rows = jnp.exp(to_end[:, None] * log_decay[None, :])
    weighted = (key_rows.astype(jnp.float32) * decay_rows[None, :, :, None]).astype(jnp.bfloat16)
    span_state = jnp.einsum(
        "sthk,sthv->shkv", weighted, value_rows, preferred_element_type=jnp.float32
    )
    carried_state = jnp.exp(log_decay * (span_len * (groups - 1 - own_index)).astype(jnp.float32))
    scaled_state = span_state * carried_state[None, :, None, None]
    state_rows = lax.psum_scatter(scaled_state, "sp", scatter_dimension=2, tiled=True)
    new_total = new_total.reshape(sequences, 1, 3, head_count, HD)
    new_position = jnp.full((1,), groups * span_len, jnp.int32)
    fresh_key = (rotate(new_total[:, :, 0], new_position) * key_scale).astype(jnp.bfloat16)[:, 0]
    new_value = new_total[:, 0, 1].astype(jnp.bfloat16)
    new_query = rotate(new_total[:, :, 2], new_position).astype(jnp.bfloat16)[:, 0]
    query_entries = new_query.astype(jnp.float32)
    decay_one = jnp.exp(log_decay)[None, :, None]
    query_share = lax.dynamic_slice_in_dim(query_entries, own_index * key_share, key_share, 2)
    partial_read = (
        jnp.einsum("shkv,shk->shv", state_rows, query_share, precision=lax.Precision.HIGHEST)
        * decay_one
    )
    summed = lax.psum(partial_read, "sp")
    own_term = jnp.sum(
        query_entries * fresh_key.astype(jnp.float32), axis=-1, keepdims=True
    ) * new_value.astype(jnp.float32)
    normed = group_norm(summed + own_term)
    return (state_rows.astype(jnp.bfloat16), normed.reshape(sequences, inner).astype(jnp.bfloat16))


def solution(mesh):
    return jax.shard_map(
        body,
        mesh=mesh,
        in_specs=(
            P(None, "sp", "tp"),
            P(None, None, "tp"),
            P(None, "tp"),
            P(None, "tp"),
            P(None, "tp"),
            P("tp"),
        ),
        out_specs=(P(None, "tp", "sp", None), P(None, "tp")),
        check_vma=False,
    )
```

profile of v0, /device:TPU:0, one launch (start us, length us, event | category | flops | bytes accessed | tf_op | source)
XLA Modules:
  0.0 200.9 jit_solution(10623617118696532471)
XLA Ops:
  7.2 0.0 all-gather.2.cloned.1.call-start
  7.2 0.7 all-gather.2.cloned.1.call-update
  7.9 0.0 reduce-scatter.2.cloned.1.call-start
  7.9 6.4 %copy.9 = bf16[4096,512]{0,1:T(8,128)(2,1)} copy(bf16[4096,512]{1,0:T(8,128)(2,1)} %param.10) | data formatting | bytes 8388608 | tf_op args[4]
  14.3 0.0 copy-start
  14.3 0.0 copy-start.1
  14.3 6.5 %copy.8 = bf16[4096,512]{0,1:T(8,128)(2,1)} copy(bf16[4096,512]{1,0:T(8,128)(2,1)} %param.9) | data formatting | bytes 8388608 | tf_op args[3]
  20.8 0.0 copy-done
  20.8 16.8 %all_gather.7 = bf16[3,1,4096]{2,0,1:T(4,128)(2,1)S(1)} all-gather(bf16[3,1,512]{2,0,1:T(4,128)(2,1)S(1)} %copy-done), channel_id=1, replica_groups=mesh['sp'=4,'tp'=8] {'tp'}, dimensions={2}, use_global_device_ids=true | all-gather | bytes 27648 | tf_op jit(solution)/shard_map/all_gather | solution.py:38
  37.7 0.0 copy-done.1
  37.7 0.1 multiply_exponential_fusion
  37.8 0.3 multiply_cosine_fusion
  38.1 91.1 %all-gather.2.cloned.1.call-done = bf16[3,512,4096]{2,1,0:T(8,128)(2,1)} async-done(((bf16[3,512,512]{2,1,0:T(8,128)(2,1)}), bf16[3,512,4096]{2,1,0:T(8,128)(2,1)}) %all-gather.2.cloned.1.call-update) | async-done | bytes 12582928 | tf_op jit(solution)/shard_map/all_gather | solution.py:37
  129.3 18.5 %fusion.7 = f32[1024,3,512]{2,0,1:T(8,128)S(1)} fusion(bf16[3,512,4096]{2,1,0:T(8,128)(2,1)} %all-gather.2.cloned.1.call-done, bf16[4096,512]{0,1:T(8,128)(2,1)} %copy.9, bf16[4096,512]{0,1:T(8,128)(2,1)} %copy.8), kind=kOutput, calls=%fused_computation.8 | convolution fusion | flops 12901679104 | bytes 27262976 | tf_op jit(solution)/shard_map/dot_general | solution.py:39
  147.8 0.3 copy_bitcast_fusion
  148.1 0.5 multiply_subtract_fusion
  148.5 1.5 fusion.20
  150.0 0.0 reduce-scatter.2.cloned.1.call-update
  150.0 5.6 %fusion.11 = f32[3,1536]{1,0:T(4,128)S(1)} fusion(bf16[4096,512]{1,0:T(8,128)(2,1)} %param.8, bf16[4096,512]{1,0:T(8,128)(2,1)} %param.10, bf16[4096,512]{1,0:T(8,128)(2,1)} %param.9, bf16[3,1,4096]{2,0,1:T(4,128)(2,1)S(1)} %all_gather.7), kind=kOutput, calls=%fused_computation.16 | convolution fusion | flops 75497472 | bytes 12625920 | tf_op jit(solution)/shard_map/dot_general | solution.py:40
  155.6 0.1 reshape.216
  155.7 0.1 multiply_sine_fusion.1
  155.8 0.1 subtract_bitcast_fusion
  155.8 0.1 fusion.31
  155.9 18.7 %reduce-scatter.2.cloned.1.call-done = f32[3,8,16,64]{3,2,1,0:T(8,128)} async-done(((f32[3,8,64,64]{3,2,1,0:T(8,128)}), f32[3,8,16,64]{3,2,1,0:T(8,128)}) %reduce-scatter.2.cloned.1.call-update) | async-done | bytes 98320 | tf_op jit(solution)/shard_map/reduce_scatter | solution.py:53
  174.6 1.1 fusion.27
  175.7 0.1 broadcast_multiply_fusion
  175.8 15.0 %psum.7 = f32[3,8,64]{2,1,0:T(8,128)S(1)} all-reduce(f32[3,8,64]{2,1,0:T(8,128)S(1)} %broadcast_multiply_fusion), channel_id=1, replica_groups=mesh['sp'=4,'tp'=8] {'sp'}, use_global_device_ids=true, to_apply=%region_1.0 | all-reduce | flops 1536 | bytes 12288 | tf_op jit(solution)/shard_map/psum | solution.py:66
  190.8 0.7 fusion.38
  191.6 0.2 multiply_reduce_fusion
  191.7 0.1 multiply_convert_fusion.4
  191.8 0.7 convert_element_type.83
  192.5 1.6 convert_element_type.76
  (7 shorter events, 0.0 us)
Async XLA Ops:
  7.2 122.1 %all-gather.2.cloned.1.call-start = ((), (), s32[]{:S(2)}) async-start(), calls=%async_computation.1 | async-start | bytes 14155776 | tf_op jit(solution)/shard_map/all_gather | solution.py:37
  7.9 166.7 %reduce-scatter.2.cloned.1.call-start = ((), (), s32[]{:S(2)}) async-start(), calls=%async_computation.2 | async-start | bytes 983040 | tf_op jit(solution)/shard_map/reduce_scatter | solution.py:53
  14.3 6.5 %copy-start = (bf16[3,1,512]{2,0,1:T(4,128)(2,1)S(1)}, bf16[3,1,512]{2,0,1:T(4,128)(2,1)}, u32[]{:S(2)}) copy-start(bf16[3,1,512]{2,0,1:T(4,128)(2,1)} %param.7) | copy-start | bytes 9220
  14.3 23.4 %copy-start.1 = (f32[8]{0:T(128)S(1)}, f32[8]{0:T(128)}, u32[]{:S(2)}) copy-start(f32[8]{0:T(128)} %param.11) | copy-start | bytes 100
Sparse Core Ops, SparseCore 0:
  9.6 119.6 all-gather.1
  150.1 24.4 reduce-scatter.1
where the time goes:
time: 201 us
  waiting for transfers between devices  110 us (55%)
  blocking collectives  31.9 us (16%)
  matrix products  26.7 us (13%)
  between operations  14.1 us (7%)
  local copies, waits for them, and re-layouts  14 us (7%)
  other arithmetic  3.69 us (2%)
    all_gather x1, waiting for transfers between devices, body(): row_piece = lax.all_gather(tokens, 'tp', axis=2, tiled=True)  91.1 us
    reduce_scatter x1, waiting for transfers between devices, body(): lax.psum_scatter(scaled_state, 'sp', scatter_dimension=2, tiled=True)  18.7 us
    dot_general x1, matrix products, body(): jnp.dot(row_piece, row_weights, preferred_element_type=jnp.float32)  18.5 us
    all_gather x1, blocking collectives, body(): new_piece = lax.all_gather(new_token, 'tp', axis=2, tiled=True)  16.8 us
    psum x1, blocking collectives, body(): summed = lax.psum(partial_read, 'sp')  15 us
    unnamed x6, local copies, waits for them, and re-layouts  12.9 us
    dot_general x1, matrix products, body(): jnp.dot(new_piece, all_weights, preferred_element_type=jnp.float32)  5.59 us
  transfers between devices with their start and end apart: 2, of which 2 were waited for; matrix products, arithmetic and copies ran while one was open for 10% of the time, Pallas kernels for 0%

commit v1 on v0

--- a/solution.py
+++ b/solution.py
@@ -34,7 +34,7 @@
     key_share = HD // groups
     row_weights = jnp.concatenate([key_weight, value_weight], axis=1)
     all_weights = jnp.concatenate([key_weight, value_weight, query_weight], axis=1)
-    row_piece = lax.all_gather(tokens, "tp", axis=2, tiled=True)
+    row_piece = jnp.concatenate(lax.all_gather(tokens, "tp"), axis=2)
     new_piece = lax.all_gather(new_token, "tp", axis=2, tiled=True)
     row_total = jnp.dot(row_piece, row_weights, preferred_element_type=jnp.float32)
     new_total = jnp.dot(new_piece, all_weights, preferred_element_type=jnp.float32)

time: 201 us -> 236 us (1.17)
  local copies, waits for them, and re-layouts: 14 us -> 47.9 us
    reshape x0 -> x1, local copies, waits for them, and re-layouts: none -> 19.6 us  [body(): row_piece = jnp.concatenate(lax.all_gather(tokens, 'tp'), axis=2)]
    all_gather x0 -> x1, local copies, waits for them, and re-layouts: none -> 14.4 us  [body(): row_piece = jnp.concatenate(lax.all_gather(tokens, 'tp'), axis=2)]
  transfers between devices with their start and end apart: 2 -> 2, of which waited for: 2 -> 2; matrix products, arithmetic and copies ran while one was open for 10% -> 8% of each run, Pallas kernels for 0% -> 0%
where the time goes in v1:
time: 236 us; the launch traced here: 235 us
  waiting for transfers between devices  110 us (47%)
  local copies, waits for them, and re-layouts  47.9 us (20%)
  blocking collectives  31.9 us (14%)
  matrix products  26.7 us (11%)
  between operations  14.1 us (6%)
  other arithmetic  3.69 us (2%)
    all_gather x1, waiting for transfers between devices, body(): row_piece = jnp.concatenate(lax.all_gather(tokens, 'tp'), axis=2)  91.1 us
    reshape x1, local copies, waits for them, and re-layouts, body(): row_piece = jnp.concatenate(lax.all_gather(tokens, 'tp'), axis=2)  19.6 us
    reduce_scatter x1, waiting for transfers between devices, body(): lax.psum_scatter(scaled_state, 'sp', scatter_dimension=2, tiled=True)  18.7 us
    dot_general x1, matrix products, body(): jnp.dot(row_piece, row_weights, preferred_element_type=jnp.float32)  18.5 us
    all_gather x1, blocking collectives, body(): new_piece = lax.all_gather(new_token, 'tp', axis=2, tiled=True)  16.9 us
    psum x1, blocking collectives, body(): summed = lax.psum(partial_read, 'sp')  15 us
    all_gather x1, local copies, waits for them, and re-layouts, body(): row_piece = jnp.concatenate(lax.all_gather(tokens, 'tp'), axis=2)  14.4 us
    unnamed x6, local copies, waits for them, and re-layouts  12.9 us
  transfers between devices with their start and end apart: 2, of which 2 were waited for; matrix products, arithmetic and copies ran while one was open for 8% of the time, Pallas kernels for 0%

profile of v1, /device:TPU:0, one launch (start us, length us, event | category | flops | bytes accessed | tf_op | source)
XLA Modules:
  0.0 234.9 jit_solution(689208947916832563)
XLA Ops:
  7.2 0.0 all-gather.3.cloned.1.call-start
  7.2 0.7 all-gather.3.cloned.1.call-update
  7.9 0.0 reduce-scatter.2.cloned.1.call-start
  7.9 6.4 %copy.15 = bf16[4096,512]{0,1:T(8,128)(2,1)} copy(bf16[4096,512]{1,0:T(8,128)(2,1)} %param.10) | data formatting | bytes 8388608 | tf_op args[4]
  14.3 0.0 copy-start
  14.3 0.0 copy-start.1
  14.3 6.5 %copy.14 = bf16[4096,512]{0,1:T(8,128)(2,1)} copy(bf16[4096,512]{1,0:T(8,128)(2,1)} %param.9) | data formatting | bytes 8388608 | tf_op args[3]
  20.8 0.0 copy-done
  20.8 16.9 %all_gather.11 = bf16[3,1,4096]{2,0,1:T(4,128)(2,1)S(1)} all-gather(bf16[3,1,512]{2,0,1:T(4,128)(2,1)S(1)} %copy-done), channel_id=1, replica_groups=mesh['sp'=4,'tp'=8] {'tp'}, dimensions={2}, use_global_device_ids=true | all-gather | bytes 27648 | tf_op jit(solution)/shard_map/all_gather | solution.py:38
  37.7 0.0 copy-done.1
  37.8 0.1 multiply_exponential_fusion
  37.8 0.3 multiply_cosine_fusion
  38.2 91.1 %all-gather.3.cloned.1.call-done = bf16[24,512,512]{2,1,0:T(8,128)(2,1)} async-done(((bf16[3,512,512]{2,1,0:T(8,128)(2,1)}), bf16[24,512,512]{2,1,0:T(8,128)(2,1)}) %all-gather.3.cloned.1.call-update) | async-done | bytes 12582928 | tf_op jit(solution)/shard_map/all_gather | solution.py:37
  129.3 14.4 %copy.35 = bf16[8,3,512,512]{3,0,2,1:T(8,128)(2,1)} copy(bf16[8,3,512,512]{3,2,1,0:T(8,128)(2,1)} %bitcast.49) | data formatting | bytes 25165824 | tf_op jit(solution)/shard_map/all_gather | solution.py:37
  143.7 19.6 %reshape.221 = bf16[3,512,4096]{2,1,0:T(8,128)(2,1)} reshape(bf16[3,512,8,512]{3,2,1,0:T(8,128)(2,1)} %bitcast.48) | data formatting | bytes 25165824 | tf_op jit(solution)/shard_map/reshape | solution.py:37
  163.3 18.5 %fusion.7 = f32[1024,3,512]{2,0,1:T(8,128)S(1)} fusion(bf16[3,512,4096]{2,1,0:T(8,128)(2,1)} %reshape.221, bf16[4096,512]{0,1:T(8,128)(2,1)} %copy.15, bf16[4096,512]{0,1:T(8,128)(2,1)} %copy.14), kind=kOutput, calls=%fused_computation.9 | convolution fusion | flops 12901679104 | bytes 27262976 | tf_op jit(solution)/shard_map/dot_general | solution.py:39
  181.8 0.3 copy_bitcast_fusion.1
  182.1 0.5 multiply_subtract_fusion
  182.5 1.5 fusion.20
  184.0 0.0 reduce-scatter.2.cloned.1.call-update
  184.0 5.6 %fusion.11 = f32[3,1536]{1,0:T(4,128)S(1)} fusion(bf16[4096,512]{1,0:T(8,128)(2,1)} %param.8, bf16[4096,512]{1,0:T(8,128)(2,1)} %param.10, bf16[4096,512]{1,0:T(8,128)(2,1)} %param.9, bf16[3,1,4096]{2,0,1:T(4,128)(2,1)S(1)} %all_gather.11), kind=kOutput, calls=%fused_computation.17 | convolution fusion | flops 75497472 | bytes 12625920 | tf_op jit(solution)/shard_map/dot_general | solution.py:40
  189.6 0.1 reshape.224
  189.7 0.1 multiply_sine_fusion.1
  189.8 0.1 subtract_bitcast_fusion
  189.9 0.1 fusion.31
  189.9 18.7 %reduce-scatter.2.cloned.1.call-done = f32[3,8,16,64]{3,2,1,0:T(8,128)} async-done(((f32[3,8,64,64]{3,2,1,0:T(8,128)}), f32[3,8,16,64]{3,2,1,0:T(8,128)}) %reduce-scatter.2.cloned.1.call-update) | async-done | bytes 98320 | tf_op jit(solution)/shard_map/reduce_scatter | solution.py:53
  208.6 1.1 fusion.27
  209.7 0.1 broadcast_multiply_fusion
  209.8 15.0 %psum.7 = f32[3,8,64]{2,1,0:T(8,128)S(1)} all-reduce(f32[3,8,64]{2,1,0:T(8,128)S(1)} %broadcast_multiply_fusion), channel_id=1, replica_groups=mesh['sp'=4,'tp'=8] {'sp'}, use_global_device_ids=true, to_apply=%region_1.0 | all-reduce | flops 1536 | bytes 12288 | tf_op jit(solution)/shard_map/psum | solution.py:66
  224.8 0.7 fusion.38
  225.5 0.2 multiply_reduce_fusion
  225.7 0.1 multiply_convert_fusion.4
  225.8 0.7 convert_element_type.83
  226.5 1.6 convert_element_type.76
  (7 shorter events, 0.0 us)
Async XLA Ops:
  7.2 122.1 %all-gather.3.cloned.1.call-start = ((), (), s32[]{:S(2)}) async-start(), calls=%async_computation.2 | async-start | bytes 14155776 | tf_op jit(solution)/shard_map/all_gather | solution.py:37
  7.9 200.7 %reduce-scatter.2.cloned.1.call-start = ((), (), s32[]{:S(2)}) async-start(), calls=%async_computation.1 | async-start | bytes 983040 | tf_op jit(solution)/shard_map/reduce_scatter | solution.py:53
  14.3 6.5 %copy-start = (bf16[3,1,512]{2,0,1:T(4,128)(2,1)S(1)}, bf16[3,1,512]{2,0,1:T(4,128)(2,1)}, u32[]{:S(2)}) copy-start(bf16[3,1,512]{2,0,1:T(4,128)(2,1)} %param.7) | copy-start | bytes 9220
  14.3 23.4 %copy-start.1 = (f32[8]{0:T(128)S(1)}, f32[8]{0:T(128)}, u32[]{:S(2)}) copy-start(f32[8]{0:T(128)} %param.11) | copy-start | bytes 100
Sparse Core Ops, SparseCore 0:
  9.6 119.6 all-gather.2
  184.1 24.4 reduce-scatter.1

commit v2 on v0

--- a/solution.py
+++ b/solution.py
@@ -63,7 +63,9 @@
         jnp.einsum("shkv,shk->shv", state_rows, query_share, precision=lax.Precision.HIGHEST)
         * decay_one
     )
-    summed = lax.psum(partial_read, "sp")
+    summed = partial_read
+    for hop in (1, 2):
+        summed = summed + lax.ppermute(summed, "sp", [(dev, dev ^ hop) for dev in range(4)])
     own_term = jnp.sum(
         query_entries * fresh_key.astype(jnp.float32), axis=-1, keepdims=True
     ) * new_value.astype(jnp.float32)

time: 201 us -> 191 us (0.950)
  blocking collectives: 31.9 us -> 16.8 us
  waiting for transfers between devices: 110 us -> 113 us
  starting transfers between devices: 0.08 us -> 3.02 us
    psum x1 -> x0, blocking collectives: 15 us -> none  [body(): summed = lax.psum(partial_read, 'sp')]
    ppermute x0 -> x2, starting transfers between devices: none -> 2.95 us  [body(): lax.ppermute(summed, 'sp', [(dev, dev ^ hop) for dev in range(4)])]
    ppermute x0 -> x2, waiting for transfers between devices: none -> 2.41 us  [body(): lax.ppermute(summed, 'sp', [(dev, dev ^ hop) for dev in range(4)])]
  transfers between devices with their start and end apart: 2 -> 4, of which waited for: 2 -> 4; matrix products, arithmetic and copies ran while one was open for 10% -> 11% of each run, Pallas kernels for 0% -> 0%
where the time goes in v2:
time: 191 us
  waiting for transfers between devices  113 us (59%)
  matrix products  26.7 us (14%)
  blocking collectives  16.8 us (9%)
  between operations  14.1 us (7%)
  local copies, waits for them, and re-layouts  14 us (7%)
  other arithmetic  3.61 us (2%)
  starting transfers between devices  3.02 us (2%)
    all_gather x1, waiting for transfers between devices, body(): row_piece = lax.all_gather(tokens, 'tp', axis=2, tiled=True)  91.1 us
    reduce_scatter x1, waiting for transfers between devices, body(): lax.psum_scatter(scaled_state, 'sp', scatter_dimension=2, tiled=True)  18.6 us
    dot_general x1, matrix products, body(): jnp.dot(row_piece, row_weights, preferred_element_type=jnp.float32)  18.5 us
    all_gather x1, blocking collectives, body(): new_piece = lax.all_gather(new_token, 'tp', axis=2, tiled=True)  16.8 us
    unnamed x6, local copies, waits for them, and re-layouts  12.9 us
    dot_general x1, matrix products, body(): jnp.dot(new_piece, all_weights, preferred_element_type=jnp.float32)  5.59 us
  transfers between devices with their start and end apart: 4, of which 4 were waited for; matrix products, arithmetic and copies ran while one was open for 11% of the time, Pallas kernels for 0%

profile of v2, /device:TPU:0, one launch (start us, length us, event | category | flops | bytes accessed | tf_op | source)
XLA Modules:
  0.0 191.1 jit_solution(6634773183823713030)
XLA Ops:
  7.2 0.0 all-gather.2.cloned.1.call-start
  7.2 0.7 all-gather.2.cloned.1.call-update
  7.9 0.0 reduce-scatter.2.cloned.1.call-start
  7.9 6.4 %copy.9 = bf16[4096,512]{0,1:T(8,128)(2,1)} copy(bf16[4096,512]{1,0:T(8,128)(2,1)} %param.10) | data formatting | bytes 8388608 | tf_op args[4]
  14.4 0.0 copy-start
  14.4 0.0 copy-start.1
  14.4 6.5 %copy.8 = bf16[4096,512]{0,1:T(8,128)(2,1)} copy(bf16[4096,512]{1,0:T(8,128)(2,1)} %param.9) | data formatting | bytes 8388608 | tf_op args[3]
  20.8 0.0 copy-done
  20.9 16.8 %all_gather.7 = bf16[3,1,4096]{2,0,1:T(4,128)(2,1)S(1)} all-gather(bf16[3,1,512]{2,0,1:T(4,128)(2,1)S(1)} %copy-done), channel_id=1, replica_groups=mesh['sp'=4,'tp'=8] {'tp'}, dimensions={2}, use_global_device_ids=true | all-gather | bytes 27648 | tf_op jit(solution)/shard_map/all_gather | solution.py:38
  37.7 0.0 copy-done.1
  37.7 0.1 multiply_exponential_fusion
  37.8 0.3 multiply_cosine_fusion
  38.1 91.1 %all-gather.2.cloned.1.call-done = bf16[3,512,4096]{2,1,0:T(8,128)(2,1)} async-done(((bf16[3,512,512]{2,1,0:T(8,128)(2,1)}), bf16[3,512,4096]{2,1,0:T(8,128)(2,1)}) %all-gather.2.cloned.1.call-update) | async-done | bytes 12582928 | tf_op jit(solution)/shard_map/all_gather | solution.py:37
  129.3 18.5 %fusion.7 = f32[1024,3,512]{2,0,1:T(8,128)S(1)} fusion(bf16[3,512,4096]{2,1,0:T(8,128)(2,1)} %all-gather.2.cloned.1.call-done, bf16[4096,512]{0,1:T(8,128)(2,1)} %copy.9, bf16[4096,512]{0,1:T(8,128)(2,1)} %copy.8), kind=kOutput, calls=%fused_computation.8 | convolution fusion | flops 12901679104 | bytes 27262976 | tf_op jit(solution)/shard_map/dot_general | solution.py:39
  147.8 0.3 copy_bitcast_fusion
  148.1 0.5 multiply_subtract_fusion
  148.5 1.5 fusion.20
  150.0 0.0 reduce-scatter.2.cloned.1.call-update
  150.0 5.6 %fusion.11 = f32[3,1536]{1,0:T(4,128)S(1)} fusion(bf16[4096,512]{1,0:T(8,128)(2,1)} %param.8, bf16[4096,512]{1,0:T(8,128)(2,1)} %param.10, bf16[4096,512]{1,0:T(8,128)(2,1)} %param.9, bf16[3,1,4096]{2,0,1:T(4,128)(2,1)S(1)} %all_gather.7), kind=kOutput, calls=%fused_computation.16 | convolution fusion | flops 75497472 | bytes 12625920 | tf_op jit(solution)/shard_map/dot_general | solution.py:40
  155.6 0.1 reshape.216
  155.7 0.1 multiply_sine_fusion.1
  155.8 0.1 subtract_convert_fusion
  155.9 0.1 fusion.30
  155.9 18.6 %reduce-scatter.2.cloned.1.call-done = f32[3,8,16,64]{3,2,1,0:T(8,128)} async-done(((f32[3,8,64,64]{3,2,1,0:T(8,128)}), f32[3,8,16,64]{3,2,1,0:T(8,128)}) %reduce-scatter.2.cloned.1.call-update) | async-done | bytes 98320 | tf_op jit(solution)/shard_map/reduce_scatter | solution.py:53
  174.5 1.1 fusion.26
  175.7 0.1 broadcast_multiply_fusion
  175.7 1.5 collective-permute-start
  177.2 2.2 %collective-permute-done = f32[3,8,64]{2,1,0:T(8,128)S(1)} collective-permute-done((f32[3,8,64]{2,1,0:T(8,128)S(1)}, f32[3,8,64]{2,1,0:T(8,128)S(1)}, u32[]{:S(2)}, u32[]{:S(2)}) %collective-permute-start) | collective-permute-done | bytes 6176 | tf_op jit(solution)/shard_map/ppermute | solution.py:68
  179.4 0.1 fusion.41
  179.5 1.5 collective-permute-start.1
  181.0 0.5 fusion.23
  181.4 1.6 convert_element_type.76
  183.0 0.2 collective-permute-done.1
  183.2 0.1 fusion.36
  183.3 0.2 multiply_reduce_fusion
  183.5 0.1 multiply_convert_fusion.4
  183.5 0.7 convert_element_type.83
  (7 shorter events, 0.0 us)
Async XLA Ops:
  7.2 122.1 %all-gather.2.cloned.1.call-start = ((), (), s32[]{:S(2)}) async-start(), calls=%async_computation.1 | async-start | bytes 14155776 | tf_op jit(solution)/shard_map/all_gather | solution.py:37
  7.9 166.6 %reduce-scatter.2.cloned.1.call-start = ((), (), s32[]{:S(2)}) async-start(), calls=%async_computation.2 | async-start | bytes 983040 | tf_op jit(solution)/shard_map/reduce_scatter | solution.py:53
  14.4 6.5 %copy-start = (bf16[3,1,512]{2,0,1:T(4,128)(2,1)S(1)}, bf16[3,1,512]{2,0,1:T(4,128)(2,1)}, u32[]{:S(2)}) copy-start(bf16[3,1,512]{2,0,1:T(4,128)(2,1)} %param.7) | copy-start | bytes 9220
  14.4 23.3 %copy-start.1 = (f32[8]{0:T(128)S(1)}, f32[8]{0:T(128)}, u32[]{:S(2)}) copy-start(f32[8]{0:T(128)} %param.11) | copy-start | bytes 100
  175.7 3.7 %collective-permute-start = (f32[3,8,64]{2,1,0:T(8,128)S(1)}, f32[3,8,64]{2,1,0:T(8,128)S(1)}, u32[]{:S(2)}, u32[]{:S(2)}) collective-permute-start(f32[3,8,64]{2,1,0:T(8,128)S(1)} %broadcast_multiply_fusion), channel_id=1, source_target_pairs={{0,8},{8,0},{16,24},{24,16},{1,9},{9,1},{17,25},{25,17},{2,10},{10... | collective-permute-start | bytes 18440 | tf_op jit(solution)/shard_map/ppermute | solution.py:68
  179.5 3.7 %collective-permute-start.1 = (f32[3,8,64]{2,1,0:T(8,128)S(1)}, f32[3,8,64]{2,1,0:T(8,128)S(1)}, u32[]{:S(2)}, u32[]{:S(2)}) collective-permute-start(f32[3,8,64]{2,1,0:T(8,128)S(1)} %fusion.41), channel_id=1, source_target_pairs={{0,16},{8,24},{16,0},{24,8},{1,17},{9,25},{17,1},{25,9},{2,18},{10... | collective-permute-start | bytes 18440 | tf_op jit(solution)/shard_map/ppermute | solution.py:68
Sparse Core Ops, SparseCore 0:
  9.6 119.6 all-gather.1
  150.1 24.3 reduce-scatter.1
